TPU v7x, 32 devices: a whole 2x2x4 slice. The times are simulated.
32 devices in a mesh: sp: 8 (over z, y), tp: 4 (over x, core).
Axes of the slice: x: 2, y: 2, z: 4, core: 2. Of those that a mesh axis runs over, the one named last changes fastest.
Arguments:
- residual_in: bfloat16 [4096, 2048], P('sp'), may hold values from -6 to 6
- queries_nope: bfloat16 [4096, 1024], P('sp', 'tp'), may hold values from -15 to 15
- queries_rope: bfloat16 [4096, 512], P('sp', 'tp'), may hold values from -400 to 400
- latents: bfloat16 [4096, 256], P('sp'), may hold values from -6 to 6
- rope_keys: bfloat16 [4096, 32], P('sp'), may hold values from -8 to 8
- latent_norm_gain: float32 [256], replicated, may hold values from 0.1 to 1.9
- key_up_weight: bfloat16 [256, 1024], P(None, 'tp'), may hold values from -0.375 to 0.375
- value_up_weight: bfloat16 [256, 1024], P(None, 'tp'), may hold values from -0.375 to 0.375
- w_out: bfloat16 [1024, 2048], P('tp'), may hold values from -0.59765625 to 0.59765625
- norm_gain: float32 [2048], replicated, may hold values from 0.1 to 1.9
- w_up: bfloat16 [2048, 8192], P('sp', 'tp'), may hold values from -0.125 to 0.125
- w_down: bfloat16 [8192, 2048], P('tp', 'sp'), may hold values from -0.0625 to 0.0625
Outputs:
- layer_out: bfloat16 [4096, 2048], P('sp', 'tp')
All inputs are finite; a program needn't handle non-finite values.
Results may differ from a plain program's by a relative error of at most 0.015.
Values may be sent and summed in bfloat16 or wider, within the bound.
A program may use at most 128 MiB of HBM per device.

v0:
```python
import math

import jax
import jax.numpy as jnp
from jax import lax
from jax.sharding import PartitionSpec as P

UNROTATED_WIDTH = 64
ROPE = 32


rope_base = 10000.0
epsilon = 1e-06


def rotate(vectors, phases):
    half_width = vectors.shape[-1] // 2
    first_half = vectors[..., :half_width]
    second_half = vectors[..., half_width:]
    cosine = jnp.cos(phases)
    sine = jnp.sin(phases)
    return jnp.concatenate(
        [first_half * cosine - second_half * sine, second_half * cosine + first_half * sine],
        axis=-1,
    )


def rope_phases(positions, width):
    inverse = 1.0 / rope_base ** (jnp.arange(0, width, 2, dtype=jnp.float32) / width)
    return positions.astype(jnp.float32)[:, None] * inverse[None, :]


def rms_scale(vectors, gain_vec):
    return (
        vectors
        * lax.rsqrt(jnp.mean(vectors * vectors, axis=-1, keepdims=True) + epsilon)
        * gain_vec
    )


def attend_block(carry, queries, key_nope, value_rows, key_rot):
    row_peak, denominator, accum = carry
    key_count = key_nope.shape[0]
    heads = queries.shape[1]
    key_all = jnp.concatenate(
        [key_nope, jnp.broadcast_to(key_rot[:, None, :], (key_count, heads, key_rot.shape[1]))],
        axis=2,
    )
    scores = jnp.einsum("qhd,khd->hqk", queries, key_all, preferred_element_type=jnp.float32) * (
        1.0 / math.sqrt(UNROTATED_WIDTH + ROPE)
    )
    new_peak = jnp.maximum(row_peak, jnp.max(scores, axis=2))
    factor = jnp.exp(row_peak - new_peak)
    weights = jnp.exp(scores - new_peak[:, :, None])
    denominator = denominator * factor + jnp.sum(weights, axis=2)
    accum = accum * jnp.transpose(factor)[:, :, None] + jnp.einsum(
        "hqk,khd->qhd", weights.astype(jnp.bfloat16), value_rows, preferred_element_type=jnp.float32
    )
    return (new_peak, denominator, accum)


def fold_blocks(carry, pieces, expand, queries):
    count = pieces[0].shape[0]
    width = math.gcd(count, 1024)

    def one_block(state, start):
        sliced = tuple((lax.dynamic_slice_in_dim(member, start, width, 0) for member in pieces))
        key_nope, value_rows, key_rot = expand(sliced)
        return attend_block(state, queries, key_nope, value_rows, key_rot)

    return lax.fori_loop(
        0, count // width, lambda turn, state: one_block(state, turn * width), carry
    )


def on_device(
    residual_in,
    queries_nope,
    queries_rope,
    latents,
    rope_keys,
    latent_norm_gain,
    key_up_weight,
    value_up_weight,
    w_out,
    norm_gain,
    w_up,
    w_down,
):
    rows = residual_in.shape[0]
    heads = key_up_weight.shape[1] // UNROTATED_WIDTH
    value_width = value_up_weight.shape[1] // heads
    positions = lax.axis_index("sp") * rows + jnp.arange(rows, dtype=jnp.int32)
    phases = rope_phases(positions, ROPE)
    q_rot = rotate(
        queries_rope.astype(jnp.float32).reshape(rows, heads, ROPE), phases[:, None, :]
    ).astype(jnp.bfloat16)
    queries = jnp.concatenate([queries_nope.reshape(rows, heads, UNROTATED_WIDTH), q_rot], axis=2)
    lat_norm = rms_scale(latents.astype(jnp.float32), latent_norm_gain).astype(jnp.bfloat16)
    key_rot = rotate(rope_keys.astype(jnp.float32), phases).astype(jnp.bfloat16)
    start_carry = (
        jnp.full((heads, rows), -1e30, jnp.float32),
        jnp.zeros((heads, rows), jnp.float32),
        jnp.zeros((rows, heads, value_width), jnp.float32),
    )

    def expand_latent(sliced):
        lat_rows, rot_rows = sliced
        count = lat_rows.shape[0]
        key_nope = (
            jnp.dot(lat_rows, key_up_weight, preferred_element_type=jnp.float32)
            .astype(jnp.bfloat16)
            .reshape(count, heads, UNROTATED_WIDTH)
        )
        value_rows = (
            jnp.dot(lat_rows, value_up_weight, preferred_element_type=jnp.float32)
            .astype(jnp.bfloat16)
            .reshape(count, heads, value_width)
        )
        return (key_nope, value_rows, rot_rows)

    result = fold_blocks(
        start_carry,
        (
            lax.all_gather(lat_norm, "sp", axis=0, tiled=True),
            lax.all_gather(key_rot, "sp", axis=0, tiled=True),
        ),
        expand_latent,
        queries,
    )
    row_peak, denominator, accum = result
    attended = (
        (accum / jnp.transpose(denominator)[:, :, None])
        .astype(jnp.bfloat16)
        .reshape(rows, heads * value_width)
    )
    part_term = jnp.dot(attended, w_out, preferred_element_type=jnp.float32)
    summed = lax.psum(part_term.astype(jnp.bfloat16), "tp").astype(jnp.float32)
    stream = residual_in.astype(jnp.float32) + summed
    normed = rms_scale(stream, norm_gain).astype(jnp.bfloat16)
    upward = jnp.dot(
        normed, lax.all_gather(w_up, "sp", axis=0, tiled=True), preferred_element_type=jnp.float32
    )
    hidden = jnp.square(jax.nn.relu(upward)).astype(jnp.bfloat16)
    terms = jnp.dot(
        hidden, lax.all_gather(w_down, "sp", axis=1, tiled=True), preferred_element_type=jnp.float32
    )
    mixer = lax.psum_scatter(
        terms.astype(jnp.bfloat16), "tp", scatter_dimension=1, tiled=True
    ).astype(jnp.float32)
    own_width = mixer.shape[1]
    own_stream = lax.dynamic_slice_in_dim(stream, lax.axis_index("tp") * own_width, own_width, 1)
    return (own_stream + mixer).astype(jnp.bfloat16)


def solution(mesh):
    in_specs = (
        P("sp", None),
        P("sp", "tp"),
        P("sp", "tp"),
        P("sp", None),
        P("sp", None),
        P(),
        P(None, "tp"),
        P(None, "tp"),
        P("tp", None),
        P(),
        P("sp", "tp"),
        P("tp", "sp"),
    )
    out_specs = P("sp", "tp")
    return jax.shard_map(
        on_device, mesh=mesh, in_specs=in_specs, out_specs=out_specs, check_vma=False
    )
```

profile of v0, /device:TPU:0, one launch (start us, length us, event | category | flops | bytes accessed | tf_op | source)
XLA Modules:
  0.0 480.2 jit_solution(10684508900544184789)
XLA Ops:
  6.5 1.2 fusion.25
  7.7 1.8 fusion.27
  9.6 0.0 all-reduce.2.cloned.1.call-start
  9.6 0.8 convert_element_type.70
  10.4 1.0 copy.15
  11.4 1.1 copy.14
  12.6 0.2 multiply_cosine_fusion
  12.8 33.2 %all_gather.13 = bf16[4096,32]{0,1:T(8,128)(2,1)S(1)} all-gather(bf16[512,32]{0,1:T(8,128)(2,1)S(1)} %pad_maximum_fusion.1), channel_id=1, replica_groups=mesh['sp'=8,'tp'=4] {'sp'}, dimensions={0}, use_global_device_ids=true | all-gather | bytes 294912 | tf_op jit(solution)/shard_map/all_gather | solution.py:126
  46.0 16.1 %all-gather.4.cloned.1.call-done = bf16[4096,256]{1,0:T(8,128)(2,1)} async-done(((bf16[512,256]{1,0:T(8,128)(2,1)}), bf16[4096,256]{1,0:T(8,128)(2,1)}) %all-gather.4.cloned.1.call-update) | async-done | bytes 2097168 | tf_op jit(solution)/shard_map/all_gather | solution.py:125
  62.1 58.6 %while.18 = (s32[]{:T(128)}, f32[4,512]{1,0:T(4,128)S(1)}, f32[4,512]{1,0:T(4,128)S(1)}, f32[512,4,64]{0,2,1:T(8,128)S(1)}, bf16[4096,256]{1,0:T(8,128)(2,1)}, /...) while((s32[]{:T(128)}, f32[4,512]{1,0:T(4,128)S(1)}, ...), condition=%wide.region_4.0_spmd.clone, body=%wide.region_1.0_spmd.clone.sunk | while | flops 958803968 | bytes 64946424 | solution.py:71
  62.1 1.4 convolution_convert_fusion.6
  63.6 4.5 bitcast_reduce_fusion.2
  68.2 1.4 convolution_convert_fusion.7
  69.6 5.1 %fusion.62 = f32[512,4,64]{0,2,1:T(8,128)S(1)} fusion(bf16[1024,4,64]{0,2,1:T(8,128)(2,1)S(1)} %bitcast.61, f32[4,1024,512]{2,1,0:T(8,128)} %get-tuple-element.285, f32[4,512]{1,0:T(4,128)S(1)} %get-tuple-element.314, f32[512,4,64]{0,2,1:T(8,128)S(1)} %get-tuple-element.303, f32[512,4]{0,1:T(4,128)S(1)} %get-tuple-element.286, pred[]{:T(512)S(6)} %compare.3), kind=kOutput, calls=%fused_computation.9.clone.1 | convolution fusion | flops 275120128 | bytes 9977857 | tf_op jit(solution)/shard_map/while/body/eval_jaxpr/hqk,khd->qhd/dot_general | solution.py:56
  74.7 0.6 copy-done.1
  75.3 1.4 fusion.60
  76.8 1.4 convolution_convert_fusion.6
  78.3 4.5 bitcast_reduce_fusion.2
  82.8 1.4 convolution_convert_fusion.7
  84.2 5.1 %fusion.62 = f32[512,4,64]{0,2,1:T(8,128)S(1)} fusion(bf16[1024,4,64]{0,2,1:T(8,128)(2,1)S(1)} %bitcast.61, f32[4,1024,512]{2,1,0:T(8,128)} %get-tuple-element.285, f32[4,512]{1,0:T(4,128)S(1)} %get-tuple-element.314, f32[512,4,64]{0,2,1:T(8,128)S(1)} %get-tuple-element.303, f32[512,4]{0,1:T(4,128)S(1)} %get-tuple-element.286, pred[]{:T(512)S(6)} %compare.3), kind=kOutput, calls=%fused_computation.9.clone.1 | convolution fusion | flops 275120128 | bytes 9977857 | tf_op jit(solution)/shard_map/while/body/eval_jaxpr/hqk,khd->qhd/dot_general | solution.py:56
  89.4 0.6 copy-done.1
  90.0 1.4 fusion.60
  91.4 1.4 convolution_convert_fusion.6
  92.9 4.5 bitcast_reduce_fusion.2
  97.5 1.4 convolution_convert_fusion.7
  98.9 5.1 %fusion.62 = f32[512,4,64]{0,2,1:T(8,128)S(1)} fusion(bf16[1024,4,64]{0,2,1:T(8,128)(2,1)S(1)} %bitcast.61, f32[4,1024,512]{2,1,0:T(8,128)} %get-tuple-element.285, f32[4,512]{1,0:T(4,128)S(1)} %get-tuple-element.314, f32[512,4,64]{0,2,1:T(8,128)S(1)} %get-tuple-element.303, f32[512,4]{0,1:T(4,128)S(1)} %get-tuple-element.286, pred[]{:T(512)S(6)} %compare.3), kind=kOutput, calls=%fused_computation.9.clone.1 | convolution fusion | flops 275120128 | bytes 9977857 | tf_op jit(solution)/shard_map/while/body/eval_jaxpr/hqk,khd->qhd/dot_general | solution.py:56
  104.0 0.6 copy-done.1
  104.6 1.4 fusion.60
  106.1 1.4 convolution_convert_fusion.6
  107.6 4.5 bitcast_reduce_fusion.2
  112.1 1.4 convolution_convert_fusion.7
  113.5 5.1 %fusion.62 = f32[512,4,64]{0,2,1:T(8,128)S(1)} fusion(bf16[1024,4,64]{0,2,1:T(8,128)(2,1)S(1)} %bitcast.61, f32[4,1024,512]{2,1,0:T(8,128)} %get-tuple-element.285, f32[4,512]{1,0:T(4,128)S(1)} %get-tuple-element.314, f32[512,4,64]{0,2,1:T(8,128)S(1)} %get-tuple-element.303, f32[512,4]{0,1:T(4,128)S(1)} %get-tuple-element.286, pred[]{:T(512)S(6)} %compare.3), kind=kOutput, calls=%fused_computation.9.clone.1 | convolution fusion | flops 275120128 | bytes 9977857 | tf_op jit(solution)/shard_map/while/body/eval_jaxpr/hqk,khd->qhd/dot_general | solution.py:56
  118.7 0.6 copy-done.1
  119.3 1.4 fusion.60
  120.7 0.1 divide_convert_fusion
  120.8 2.1 convolution_convert_fusion.2
  122.9 0.0 all-gather.6.cloned.1.call-start
  123.0 0.7 all-gather.6.cloned.1.call-update
  123.7 0.0 all-gather.8.cloned.1.call-start
  123.7 0.5 all-gather.8.cloned.1.call-update
  124.3 0.2 reduce-scatter.2.cloned.1.call-start
  124.5 48.9 %all-reduce.2.cloned.1.call-done = bf16[512,2048]{1,0:T(8,128)(2,1)} async-done(((bf16[512,2048]{1,0:T(8,128)(2,1)}), bf16[512,2048]{1,0:T(8,128)(2,1)}) %all-reduce.2.cloned.1.call-update) | async-done | bytes 2097168 | tf_op jit(solution)/shard_map/psum | solution.py:138
  173.4 4.2 convert_add_fusion
  177.6 122.5 %all-gather.6.cloned.1.call-done = bf16[2048,2048]{1,0:T(8,128)(2,1)} async-done(((bf16[256,2048]{1,0:T(8,128)(2,1)}), bf16[2048,2048]{1,0:T(8,128)(2,1)}) %all-gather.6.cloned.1.call-update) | async-done | bytes 8388624 | tf_op jit(solution)/shard_map/all_gather | solution.py:142
  300.1 125.0 %all-gather.8.cloned.1.call-done = bf16[2048,2048]{1,0:T(8,128)(2,1)} async-done(((bf16[2048,256]{1,0:T(8,128)(2,1)}), bf16[2048,2048]{1,0:T(8,128)(2,1)}) %all-gather.8.cloned.1.call-update) | async-done | bytes 8388624 | tf_op jit(solution)/shard_map/all_gather | solution.py:146
  425.2 16.6 %convolution_convert_fusion.3 = bf16[512,2048]{1,0:T(8,128)(2,1)} fusion(bf16[2048,2048]{1,0:T(8,128)(2,1)} %all-gather.8.cloned.1.call-done, bf16[2048,2048]{1,0:T(8,128)(2,1)} %all-gather.6.cloned.1.call-done, f32[2048]{0:T(1024)S(1)} %copy-done.4, f32[512]{0:T(512)S(1)} %add_rsqrt_fusion, bf16[512,2048]{1,0:T(8,128)(2,1)} %all-reduce.2.cloned.1.call-done, ...), kind=kOutput, calls=%fused_computation.32 | convolution fusion | flops 8600420352 | bytes 23078912 | tf_op jit(solution)/shard_map/dot_general | solution.py:145
  441.8 29.5 %reduce-scatter.2.cloned.1.call-done = bf16[512,512]{1,0:T(8,128)(2,1)} async-done(((bf16[512,2048]{1,0:T(8,128)(2,1)}), bf16[512,512]{1,0:T(8,128)(2,1)}) %reduce-scatter.2.cloned.1.call-update) | async-done | bytes 524304 | tf_op jit(solution)/shard_map/reduce_scatter | solution.py:148
  471.3 2.3 add_convert_fusion
  (52 shorter events, 0.5 us)
Async XLA Ops:
  6.5 114.3 %copy-start = (bf16[256,2048]{1,0:T(8,128)(2,1)S(1)}, bf16[256,2048]{1,0:T(8,128)(2,1)}, u32[]{:S(2)}) copy-start(bf16[256,2048]{1,0:T(8,128)(2,1)} %param.22) | copy-start | bytes 3145732
  6.5 55.6 %all-gather.4.cloned.1.call-start = ((), (), s32[]{:S(2)}) async-start(), calls=%async_computation.1 | async-start | bytes 2359296 | tf_op jit(solution)/shard_map/all_gather | solution.py:125
  9.6 163.9 %all-reduce.2.cloned.1.call-start = ((), (), s32[]{:S(2)}) async-start(), calls=%async_computation.2 | async-start | bytes 4194304 | tf_op jit(solution)/shard_map/psum | solution.py:138
  63.6 4.6 copy-start.2
  69.6 5.8 %copy-start.1 = (f32[4,1024,512]{2,1,0:T(8,128)S(1)}, f32[4,1024,512]{2,1,0:T(8,128)}, u32[]{:S(2)}) copy-start(f32[4,1024,512]{2,1,0:T(8,128)} %get-tuple-element.285) | copy-start | bytes 25165828 | tf_op jit(solution)/shard_map/while
  78.2 4.6 copy-start.2
  84.2 5.8 %copy-start.1 = (f32[4,1024,512]{2,1,0:T(8,128)S(1)}, f32[4,1024,512]{2,1,0:T(8,128)}, u32[]{:S(2)}) copy-start(f32[4,1024,512]{2,1,0:T(8,128)} %get-tuple-element.285) | copy-start | bytes 25165828 | tf_op jit(solution)/shard_map/while
  92.9 4.6 copy-start.2
  98.9 5.8 %copy-start.1 = (f32[4,1024,512]{2,1,0:T(8,128)S(1)}, f32[4,1024,512]{2,1,0:T(8,128)}, u32[]{:S(2)}) copy-start(f32[4,1024,512]{2,1,0:T(8,128)} %get-tuple-element.285) | copy-start | bytes 25165828 | tf_op jit(solution)/shard_map/while
  107.5 4.6 copy-start.2
  113.5 5.8 %copy-start.1 = (f32[4,1024,512]{2,1,0:T(8,128)S(1)}, f32[4,1024,512]{2,1,0:T(8,128)}, u32[]{:S(2)}) copy-start(f32[4,1024,512]{2,1,0:T(8,128)} %get-tuple-element.285) | copy-start | bytes 25165828 | tf_op jit(solution)/shard_map/while
  120.8 52.6 %copy-start.3 = (bf16[512,2048]{1,0:T(8,128)(2,1)S(1)}, bf16[512,2048]{1,0:T(8,128)(2,1)}, u32[]{:S(2)}) copy-start(bf16[512,2048]{1,0:T(8,128)(2,1)} %param.14) | copy-start | bytes 6291460
  122.9 177.2 %all-gather.6.cloned.1.call-start = ((), (), s32[]{:S(2)}) async-start(), calls=%async_computation.3 | async-start | bytes 9437184 | tf_op jit(solution)/shard_map/all_gather | solution.py:142
  123.7 301.5 %all-gather.8.cloned.1.call-start = ((), (), s32[]{:S(2)}) async-start(), calls=%async_computation.4 | async-start | bytes 9437184 | tf_op jit(solution)/shard_map/all_gather | solution.py:146
  124.2 300.9 %copy-start.4 = (f32[2048]{0:T(1024)S(1)}, f32[2048]{0:T(1024)}, u32[]{:S(2)}) copy-start(f32[2048]{0:T(1024)} %param.23) | copy-start | bytes 24580
  124.3 347.1 %reduce-scatter.2.cloned.1.call-start = ((), (), s32[]{:S(2)}) async-start(), calls=%async_computation.5 | async-start | bytes 2621440 | tf_op jit(solution)/shard_map/reduce_scatter | solution.py:148
Sparse Core Ops, SparseCore 0:
  9.7 52.4 all-gather.3
  123.0 50.3 all-reduce.1
  175.6 124.5 all-gather.5
  302.0 123.1 all-gather.7
  441.9 29.3 reduce-scatter.1
where the time goes:
time: 481 us; the launch traced here: 480 us
  waiting for transfers between devices  343 us (71%)
  matrix products  68.6 us (14%)
  blocking collectives  33.2 us (7%)
  other arithmetic  16.3 us (3%)
  between operations  13.3 us (3%)
    all_gather x1, waiting for transfers between devices, on_device(): lax.all_gather(w_down, 'sp', axis=1, tiled=True)  125 us
    all_gather x1, waiting for transfers between devices, on_device(): lax.all_gather(w_up, 'sp', axis=0, tiled=True)  123 us
    psum x1, waiting for transfers between devices, on_device(): summed = lax.psum(part_term.astype(jnp.bfloat16), 'tp').astype(jnp.float32)  48.9 us
    all_gather x1, blocking collectives, on_device(): lax.all_gather(key_rot, 'sp', axis=0, tiled=True)  33.2 us
    reduce_scatter x1, waiting for transfers between devices, on_device(): lax.psum_scatter(terms.astype(jnp.bfloat16), 'tp', scatter_dimension=1, t...  29.5 us
    dot_general x4, matrix products, attend_block(): jnp.einsum('hqk,khd->qhd', weights.astype(jnp.bfloat16), value_rows, pref...  20.6 us
    dot_general x4, matrix products, attend_block(): jnp.einsum('qhd,khd->hqk', queries, key_all, preferred_element_type=jnp.f...  18.2 us
    dot_general x1, matrix products, on_device(): jnp.dot(hidden, lax.all_gather(w_down, 'sp', axis=1, tiled=True), preferr...  16.6 us
  transfers between devices with their start and end apart: 5, of which 5 were waited for; matrix products, arithmetic and copies ran while one was open for 2% of the time, Pallas kernels for 0%

commit v1 on v0

v1 whole, which is shorter than its diff:
```python
import functools
import math

import jax
import jax.numpy as jnp
from jax import lax
from jax.experimental import pallas as pl
from jax.experimental.pallas import tpu as pltpu
from jax.sharding import PartitionSpec as P

UNROTATED_WIDTH = 64
ROPE = 32
LANES = 128

rope_base = 10000.0
epsilon = 1e-06
F32 = jnp.float32
BF16 = jnp.bfloat16
MESH = pl.DeviceIdType.MESH
NT = (((1,), (1,)), ((), ()))


def rotate(vectors, phases):
    half_width = vectors.shape[-1] // 2
    first_half = vectors[..., :half_width]
    second_half = vectors[..., half_width:]
    cosine = jnp.cos(phases)
    sine = jnp.sin(phases)
    return jnp.concatenate(
        [first_half * cosine - second_half * sine, second_half * cosine + first_half * sine],
        axis=-1,
    )


def rope_phases(positions, width):
    inverse = 1.0 / rope_base ** (jnp.arange(0, width, 2, dtype=jnp.float32) / width)
    return positions.astype(jnp.float32)[:, None] * inverse[None, :]


def rms_scale(vectors, gain_vec):
    return (
        vectors
        * lax.rsqrt(jnp.mean(vectors * vectors, axis=-1, keepdims=True) + epsilon)
        * gain_vec
    )


def ring_of(index, n):
    return index // 2 + (index % 2) * (n - 1 - 2 * (index // 2))


def index_of(place, n):
    return 2 * place + (place // (n // 2)) * (2 * n - 1 - 4 * place)


def ring_ids(n):
    place = ring_of(lax.axis_index("sp"), n)

    def at(offset):
        return index_of((place + offset + 2 * n) % n, n)

    return at


def attention_kernel(
    n, heads, scale, q_ref, x_ref, wk_ref, wv_ref, wo_ref, wu_ref,
    part_ref, full_ref,
    xs, peak, acc, xsend, xrecv, wsend, wrecv, own_sem,
):
    at = ring_ids(n)
    tp = lax.axis_index("tp")
    me = lax.axis_index("sp")
    to = ((at(1), tp), (at(-1), tp))
    barrier = pltpu.get_barrier_semaphore()
    for target in to:
        pl.semaphore_signal(barrier, inc=1, device_id=target, device_id_type=MESH)
    pl.semaphore_wait(barrier, 2)

    latent = wk_ref.shape[1]
    value_width = wv_ref.shape[0] // heads

    def x_copy(step, half, src):
        return pltpu.make_async_remote_copy(
            src_ref=src, dst_ref=xs.at[step + 1, half],
            send_sem=xsend.at[step, half], recv_sem=xrecv.at[step, half],
            device_id=to[half], device_id_type=MESH,
        )

    def w_copy(step, half, src):
        owner = at(-step) if half == 0 else at(step)
        return pltpu.make_async_remote_copy(
            src_ref=full_ref.at[owner, half] if src is None else src,
            dst_ref=full_ref.at[owner, half],
            send_sem=wsend.at[step, half], recv_sem=wrecv.at[step, half],
            device_id=to[half], device_id_type=MESH,
        )

    for half in range(2):
        x_copy(0, half, x_ref.at[half]).start()
    for half in range(2):
        w_copy(0, half, wu_ref.at[half]).start()
    own = pltpu.make_async_copy(wu_ref, full_ref.at[me], own_sem)
    own.start()
    peak[...] = jnp.full(peak.shape, -1e30, F32)
    acc[...] = jnp.zeros(acc.shape, F32)

    def attend(block_a, block_b):
        block = jnp.concatenate([block_a, block_b], axis=1)
        lat = block[:latent]
        rot = block[latent:]
        keys = block.shape[1]
        k_all = jnp.dot(wk_ref[...], lat, preferred_element_type=F32).astype(BF16)
        v_all = jnp.dot(wv_ref[...], lat, preferred_element_type=F32).astype(BF16)
        k_pad = jnp.zeros((LANES - UNROTATED_WIDTH - rot.shape[0], keys), BF16)
        ones = jnp.ones((16, keys), BF16)
        v_pad = jnp.zeros((LANES - value_width - 16, keys), BF16)
        for h in range(heads):
            k_h = jnp.concatenate(
                [k_all[h * UNROTATED_WIDTH:(h + 1) * UNROTATED_WIDTH], rot, k_pad], axis=0)
            v_h = jnp.concatenate(
                [v_all[h * value_width:(h + 1) * value_width], ones, v_pad], axis=0)
            s = jnp.dot(q_ref[:, h * LANES:(h + 1) * LANES], k_h, preferred_element_type=F32)
            old = peak[h]
            new = jnp.maximum(old, jnp.max(s, axis=1, keepdims=True))
            p = jnp.exp2((s - new) * scale).astype(BF16)
            acc[h] = acc[h] * jnp.exp2((old - new) * scale) + lax.dot_general(
                p, v_h, NT, preferred_element_type=F32)
            peak[h] = new

    attend(x_ref[0], x_ref[1])

    def turn(i, carry):
        for half in range(2):
            x_copy(i - 1, half, x_ref.at[half]).wait_recv()

            @pl.when(i < n - 1)
            def _():
                x_copy(i, half, xs.at[i, half]).start()

        for half in range(2):
            w_copy(i - 1, half, wu_ref.at[half]).wait_recv()

            @pl.when(i < n - 1)
            def _():
                w_copy(i, half, None).start()

        attend(xs[i, 0], xs[i, 1])
        return carry

    lax.fori_loop(1, n, turn, 0)

    width = part_ref.shape[2]
    group = []
    for h in range(heads):
        a = acc[h]
        group.append((a[:, :value_width] / a[:, value_width:value_width + 1]).astype(BF16))
    attended = jnp.concatenate(group, axis=1)
    for j in range(part_ref.shape[0]):
        part_ref[j] = jnp.dot(
            attended, wo_ref[:, j * width:(j + 1) * width], preferred_element_type=F32
        ).astype(BF16)

    own.wait()

    def drain(i, carry):
        for half in range(2):
            x_copy(i, half, x_ref.at[half]).wait_send()
            w_copy(i, half, wu_ref.at[half]).wait_send()
        return carry

    lax.fori_loop(0, n - 1, drain, 0)


def feed_kernel(
    n, n_tp, narrow, part_ref, res_ref, gain_ref, up_hbm, wd_ref,
    out_ref,
    up, down, parts, ys, sq, own_stream, hidden, pieces, fin,
    dsend, drecv, psend, precv, ysend, yrecv, qsend, qrecv, fsend, frecv, local,
):
    at = ring_ids(n)
    tp = lax.axis_index("tp")
    sp = lax.axis_index("sp")
    to = ((at(1), tp), (at(-1), tp))
    peers = [(tp + k) % n_tp for k in range(1, n_tp)]
    barrier = pltpu.get_barrier_semaphore()
    for target in list(to) + [(sp, p) for p in peers]:
        pl.semaphore_signal(barrier, inc=1, device_id=target, device_id_type=MESH)
    pl.semaphore_wait(barrier, 2 + n_tp - 1)

    rows, width = res_ref.shape
    per = n // n_tp

    def d_copy(step, half, src):
        return pltpu.make_async_remote_copy(
            src_ref=down.at[step, half] if src is None else src,
            dst_ref=down.at[step + 1, half],
            send_sem=dsend.at[step, half], recv_sem=drecv.at[step, half],
            device_id=to[half], device_id_type=MESH,
        )

    def p_copy(k):
        peer = peers[k]
        return pltpu.make_async_remote_copy(
            src_ref=part_ref.at[peer], dst_ref=parts.at[k],
            send_sem=psend.at[k], recv_sem=precv.at[k],
            device_id=(sp, peer), device_id_type=MESH,
        )

    def y_copy(k):
        return pltpu.make_async_remote_copy(
            src_ref=ys.at[tp], dst_ref=ys.at[tp],
            send_sem=ysend.at[k], recv_sem=yrecv.at[k],
            device_id=(sp, peers[k]), device_id_type=MESH,
        )

    def q_copy(k):
        return pltpu.make_async_remote_copy(
            src_ref=sq.at[0], dst_ref=sq.at[k + 1],
            send_sem=qsend.at[k], recv_sem=qrecv.at[k],
            device_id=(sp, peers[k]), device_id_type=MESH,
        )

    def event(step):
        for half in range(2):
            d_copy(step - 1, half, wd_ref.at[half]).wait_recv()
            d_copy(step, half, None).start()

    for half in range(2):
        d_copy(0, half, wd_ref.at[half]).start()
    for k in range(n_tp - 1):
        p_copy(k).start()
    load = pltpu.make_async_copy(up_hbm, up, local.at[0])
    load.start()
    early = min(n - 2, 5)

    def maybe(step):
        if step <= early:
            event(step)

    maybe(1)
    for k in range(n_tp - 1):
        p_copy(k).wait_recv()
    maybe(2)
    stream = part_ref[tp].astype(F32)
    for k in range(n_tp - 1):
        stream = stream + parts[k].astype(F32)
    stream = stream + res_ref[...].astype(F32)
    own_stream[...] = stream
    ys[tp] = (stream * gain_ref[...]).astype(BF16)
    total = jnp.sum(stream * stream, axis=1, keepdims=True)
    sq[0] = jnp.transpose(jnp.broadcast_to(total, (rows, LANES)))[:8]
    for k in range(n_tp - 1):
        q_copy(k).start()
        y_copy(k).start()
    maybe(3)
    for k in range(n_tp - 1):
        q_copy(k).wait_recv()
    for k in range(n_tp - 1):
        pltpu.make_async_remote_copy(
            src_ref=ys.at[tp], dst_ref=ys.at[(tp + n_tp - 1 - k) % n_tp],
            send_sem=ysend.at[k], recv_sem=yrecv.at[k],
            device_id=(sp, peers[k]), device_id_type=MESH,
        ).wait_recv()
    maybe(4)
    squares = sq[0]
    for k in range(1, n_tp):
        squares = squares + sq[k]
    squares = jnp.concatenate([squares] * (LANES // 8), axis=0)
    factor = lax.rsqrt(jnp.transpose(squares)[:, :1] / (width * n_tp) + epsilon)
    load.wait()
    units = hidden.shape[1]
    tile = math.gcd(units, 512)

    def up_step(c, carry):
        columns = pl.ds(pl.multiple_of(c * tile, tile), tile)
        total = jnp.dot(ys[0], up[:width, columns], preferred_element_type=F32)
        for t in range(1, n_tp):
            total = total + jnp.dot(
                ys[t], up[t * width:(t + 1) * width, columns], preferred_element_type=F32)
        total = jnp.maximum(total, 0.0) * factor
        hidden[:, columns] = (total * total).astype(BF16)
        return carry

    lax.fori_loop(0, units // tile, up_step, 0)
    maybe(5)

    def owners(i):
        return at(-i), at(i)

    def f_copy(i, half, owner):
        return pltpu.make_async_remote_copy(
            src_ref=pieces.at[i, half],
            dst_ref=fin.at[tp, owner % per, half],
            send_sem=fsend.at[i, half], recv_sem=frecv.at[tp, owner % per, half],
            device_id=(sp, owner // per), device_id_type=MESH,
        )

    def down_block(i, left, right):
        if narrow:
            block = jnp.concatenate([left, right], axis=0)
            half_width = left.shape[0]
            term = lax.dot_general(hidden[...], block, NT, preferred_element_type=F32)
        else:
            block = jnp.concatenate([left, right], axis=1)
            half_width = left.shape[1]
            term = jnp.dot(hidden[...], block, preferred_element_type=F32)
        term = term.astype(BF16)
        pieces[i, 0] = term[:, :half_width]
        pieces[i, 1] = term[:, half_width:]
        for half, owner in enumerate(owners(i)):

            @pl.when(owner // per != tp)
            def _():
                f_copy(i, half, owner).start()

            @pl.when(owner // per == tp)
            def _():
                fin[tp, owner % per, half] = pieces[i, half]

    down_block(0, wd_ref[0], wd_ref[1])

    def down_step(i, carry):
        @pl.when(i > early)
        def _():
            for half in range(2):
                d_copy(i - 1, half, wd_ref.at[half]).wait_recv()

        @pl.when(jnp.logical_and(i > early, i < n - 1))
        def _():
            for half in range(2):
                d_copy(i, half, None).start()

        down_block(i, down[i, 0], down[i, 1])
        return carry

    lax.fori_loop(1, n, down_step, 0)

    for k in range(n_tp - 1):
        source = (tp + n_tp - 1 - k) % n_tp
        for o in range(per):
            for half in range(2):
                pltpu.make_async_remote_copy(
                    src_ref=pieces.at[0, half], dst_ref=fin.at[source, o, half],
                    send_sem=fsend.at[0, half], recv_sem=frecv.at[source, o, half],
                    device_id=(sp, peers[k]), device_id_type=MESH,
                ).wait_recv()
    piece = fin.shape[4]
    for o in range(per):
        for half in range(2):
            start = (2 * o + half) * piece
            total = own_stream[:, start:start + piece]
            mixed = fin[0, o, half].astype(F32)
            for t in range(1, n_tp):
                mixed = mixed + fin[t, o, half].astype(F32)
            out_ref[:, start:start + piece] = (total + mixed).astype(BF16)

    def drain(i, carry):
        for half in range(2):
            d_copy(i, half, wd_ref.at[half]).wait_send()
        return carry

    lax.fori_loop(0, n - 1, drain, 0)

    def drain_pieces(i, carry):
        for half, owner in enumerate(owners(i)):

            @pl.when(owner // per != tp)
            def _():
                f_copy(i, half, owner).wait_send()

        return carry

    lax.fori_loop(0, n, drain_pieces, 0)
    for k in range(n_tp - 1):
        p_copy(k).wait_send()
        q_copy(k).wait_send()
        y_copy(k).wait_send()


def vmem():
    return pl.BlockSpec(memory_space=pltpu.VMEM)


def hbm():
    return pl.BlockSpec(memory_space=pl.ANY)


def on_device(
    n,
    n_tp,
    residual_in,
    queries_nope,
    queries_rope,
    latents,
    rope_keys,
    latent_norm_gain,
    key_up_weight,
    value_up_weight,
    w_out,
    norm_gain,
    w_up,
    w_down,
):
    rows, model = residual_in.shape
    heads = key_up_weight.shape[1] // UNROTATED_WIDTH
    value_width = value_up_weight.shape[1] // heads
    positions = lax.axis_index("sp") * rows + jnp.arange(rows, dtype=jnp.int32)
    phases = rope_phases(positions, ROPE)
    q_rot = rotate(
        queries_rope.astype(F32).reshape(rows, heads, ROPE), phases[:, None, :]
    ).astype(BF16)
    queries = jnp.concatenate(
        [
            queries_nope.reshape(rows, heads, UNROTATED_WIDTH),
            q_rot,
            jnp.zeros((rows, heads, LANES - UNROTATED_WIDTH - ROPE), BF16),
        ],
        axis=2,
    ).reshape(rows, heads * LANES)
    lat_norm = rms_scale(latents.astype(F32), latent_norm_gain).astype(BF16)
    key_rot = rotate(rope_keys.astype(F32), phases).astype(BF16)
    x = jnp.concatenate([lat_norm, key_rot], axis=1)
    wide = x.shape[1]
    x = jnp.transpose(x.reshape(2, rows // 2, wide), (0, 2, 1))

    width = model // n_tp
    depth, units = w_up.shape
    dma = pltpu.SemaphoreType.DMA
    part, full = pl.pallas_call(
        functools.partial(
            attention_kernel, n, heads,
            math.log2(math.e) / math.sqrt(UNROTATED_WIDTH + ROPE)),
        out_shape=(
            jax.ShapeDtypeStruct((n_tp, rows, width), BF16),
            jax.ShapeDtypeStruct((n, 2, depth // 2, units), BF16),
        ),
        in_specs=[vmem()] * 5 + [hbm()],
        out_specs=(vmem(), hbm()),
        scratch_shapes=[
            pltpu.VMEM((n, 2, wide, rows // 2), BF16),
            pltpu.VMEM((heads, rows, 1), F32),
            pltpu.VMEM((heads, rows, LANES), F32),
            dma((n - 1, 2)), dma((n - 1, 2)), dma((n - 1, 2)), dma((n - 1, 2)), dma,
        ],
        compiler_params=pltpu.CompilerParams(
            collective_id=0, has_side_effects=True, vmem_limit_bytes=56 * 2**20),
        name="attend",
    )(
        queries, x, jnp.transpose(key_up_weight), jnp.transpose(value_up_weight),
        w_out, w_up.reshape(2, depth // 2, units),
    )

    hidden_units, share = w_down.shape
    narrow = (share // 2) % LANES != 0
    halves = jnp.transpose(
        w_down.reshape(hidden_units, 2, share // 2), (1, 2, 0) if narrow else (1, 0, 2))
    t = lax.axis_index("tp")
    own_residual = lax.dynamic_slice_in_dim(residual_in, t * width, width, 1)
    own_gain = lax.dynamic_slice_in_dim(norm_gain, t * width, width, 0)[None, :]
    per = n // n_tp
    return pl.pallas_call(
        functools.partial(feed_kernel, n, n_tp, narrow),
        out_shape=jax.ShapeDtypeStruct((rows, width), BF16),
        in_specs=[vmem()] * 3 + [hbm(), vmem()],
        out_specs=vmem(),
        scratch_shapes=[
            pltpu.VMEM((model, units), BF16),
            pltpu.VMEM((n,) + halves.shape, BF16),
            pltpu.VMEM((n_tp - 1, rows, width), BF16),
            pltpu.VMEM((n_tp, rows, width), BF16),
            pltpu.VMEM((n_tp, 8, rows), F32),
            pltpu.VMEM((rows, width), F32),
            pltpu.VMEM((rows, units), BF16),
            pltpu.VMEM((n, 2, rows, share // 2), BF16),
            pltpu.VMEM((n_tp, per, 2, rows, share // 2), BF16),
            dma((n - 1, 2)), dma((n - 1, 2)),
            dma((n_tp - 1,)), dma((n_tp - 1,)),
            dma((n_tp - 1,)), dma((n_tp - 1,)),
            dma((n_tp - 1,)), dma((n_tp - 1,)),
            dma((n, 2)), dma((n_tp, per, 2)),
            dma((1,)),
        ],
        compiler_params=pltpu.CompilerParams(
            collective_id=1, has_side_effects=True, vmem_limit_bytes=60 * 2**20),
        name="feed",
    )(part, own_residual, own_gain, full.reshape(model, units), halves)


def solution(mesh):
    in_specs = (
        P("sp", None),
        P("sp", "tp"),
        P("sp", "tp"),
        P("sp", None),
        P("sp", None),
        P(),
        P(None, "tp"),
        P(None, "tp"),
        P("tp", None),
        P(),
        P("sp", "tp"),
        P("tp", "sp"),
    )
    out_specs = P("sp", "tp")
    return jax.shard_map(
        functools.partial(on_device, mesh.shape["sp"], mesh.shape["tp"]),
        mesh=mesh, in_specs=in_specs, out_specs=out_specs, check_vma=False,
    )
```

time: 481 us -> 230 us (0.48)
  waiting for transfers between devices: 343 us -> 0 us
  Pallas kernels: 0 us -> 215 us
  matrix products: 68.6 us -> 0 us
  blocking collectives: 33.2 us -> 0 us
  other arithmetic: 16.3 us -> 1.75 us
  between operations: 13.3 us -> 0.16 us
  local copies, waits for them, and re-layouts: 4.7 us -> 12.7 us
    all_gather x3 -> x0, waiting for transfers between devices: 264 us -> none  [the longest x1 125 us: on_device(): lax.all_gather(w_down, 'sp', axis=1, tiled=True)]
    pallas_call x0 -> x2, Pallas kernels: none -> 215 us  [the longest x1 114 us: on_device(): pl.pallas_call(functools.partial(attention_kernel, n, heads, math.log2(ma...]
    dot_general x18 -> x0, matrix products: 68.6 us -> none  [the longest x4 20.6 us: attend_block(): jnp.einsum('hqk,khd->qhd', weights.astype(jnp.bfloat16), value_rows, pref...]
    psum x1 -> x0, waiting for transfers between devices: 48.9 us -> none  [on_device(): summed = lax.psum(part_term.astype(jnp.bfloat16), 'tp').astype(jnp.float32)]
    all_gather x1 -> x0, blocking collectives: 33.2 us -> none  [on_device(): lax.all_gather(key_rot, 'sp', axis=0, tiled=True)]
    reduce_scatter x1 -> x0, waiting for transfers between devices: 29.5 us -> none  [on_device(): lax.psum_scatter(terms.astype(jnp.bfloat16), 'tp', scatter_dimension=1, t...]
    unnamed x7 -> x16, local copies, waits for them, and re-layouts: 1.11 us -> 7 us
    reduce_sum x4 -> x0, other arithmetic: 5.55 us -> none  [attend_block(): denominator = denominator * factor + jnp.sum(weights, axis=2)]
  transfers between devices with their start and end apart: 5 -> 0, of which waited for: 5 -> 0; matrix products, arithmetic and copies ran while one was open for 2% -> 0% of each run, Pallas kernels for 0% -> 0%
where the time goes in v1:
time: 230 us
  Pallas kernels  215 us (93%)
  local copies, waits for them, and re-layouts  12.7 us (6%)
    pallas_call x1, Pallas kernels, on_device(): pl.pallas_call(functools.partial(attention_kernel, n, heads, math.log2(ma...  114 us
    pallas_call x1, Pallas kernels, on_device(): pl.pallas_call(functools.partial(feed_kernel, n, n_tp, narrow), out_shape...  102 us
    unnamed x16, local copies, waits for them, and re-layouts  7 us

profile of v1, /device:TPU:0, one launch (start us, length us, event | category | flops | bytes accessed | tf_op | source)
XLA Modules:
  0.0 230.1 jit_solution(14073839040786412871)
XLA Ops:
  0.0 0.0 copy-start
  0.0 0.0 copy-start.1
  0.0 0.9 convert_element_type.22
  0.9 0.2 subtract_convert_fusion.1
  1.2 0.0 copy-start.4
  1.2 1.0 copy.20
  2.3 1.1 copy.19
  3.4 0.1 pad.6.clone
  3.4 0.1 maximum_maximum_fusion
  3.6 0.0 copy-start.2
  3.6 0.0 copy-start.3
  3.6 1.0 copy.30.q_ref
  4.6 0.1 copy.22
  4.7 0.1 copy.23
  4.9 0.0 copy-done.1
  4.9 0.1 fusion
  5.1 0.0 copy-done.4
  5.1 0.1 fusion.2
  5.2 0.1 pad_maximum_fusion
  5.3 0.9 copy.25
  6.2 0.0 copy-done.2
  6.2 0.8 copy.26
  7.0 0.0 copy-done.3
  7.0 0.8 copy.27
  7.7 113.9 %attend.1 = (bf16[4,512,512]{2,1,0:T(8,128)(2,1)}, bf16[8,2,128,2048]{3,2,1,0:T(8,128)(2,1)}) custom-call(bf16[512,512]{1,0:T(8,128)(2,1)} %copy.30.q_ref, bf16[2,288,256]{2,1,0:T(8,128)(2,1)} %bitcast.18, bf16[256,256]{1,0:T(8,128)(2,1)} %bitcast.21, bf16[256,256]{1,0:T(8,128)(2,1)} %bitcast.22, bf16[256,2048]{1,0:T(8,128)(2,1)} %wo_ref.1, ...), custom_call_target="tpu_custom_call" | custom-call | tf_op jit(solution)/shard_map/attend/pallas_call | solution.py:429
  121.6 0.0 copy-done
  121.7 0.8 constant_dynamic-slice_fusion.res_ref
  122.5 1.4 dynamic_slice.7
  123.9 1.5 copy.28
  125.3 1.3 copy.29
  126.7 101.5 %feed.1 = bf16[512,512]{1,0:T(8,128)(2,1)} custom-call(bf16[4,512,512]{2,1,0:T(8,128)(2,1)} %get-tuple-element.7.part_ref, bf16[512,512]{1,0:T(8,128)(2,1)} %constant_dynamic-slice_fusion.res_ref, f32[1,512]{1,0:T(1,128)} %bitcast.24, bf16[2048,2048]{1,0:T(8,128)(2,1)} %bitcast.13, bf16[2,2048,128]{2,1,0:T(8,128)(2,1)} %bitcast.15), custom_call_target="tpu_custom_call" | custom-call | tf_op jit(solution)/shard_map/feed/pallas_call | solution.py:461
  228.2 1.9 copy.34
  (6 shorter events, 0.1 us)
Async XLA Ops:
  0.0 121.6 %copy-start = (bf16[512,2048]{1,0:T(8,128)(2,1)S(1)}, bf16[512,2048]{1,0:T(8,128)(2,1)}, u32[]{:S(2)}) copy-start(bf16[512,2048]{1,0:T(8,128)(2,1)} %param.12) | copy-start | bytes 6291460
  0.0 4.9 %copy-start.1 = (bf16[512,256]{1,0:T(8,128)(2,1)S(1)}, bf16[512,256]{1,0:T(8,128)(2,1)}, u32[]{:S(2)}) copy-start(bf16[512,256]{1,0:T(8,128)(2,1)} %param.15) | copy-start | bytes 786436
  1.2 3.9 %copy-start.4 = (f32[256]{0:T(256)S(1)}, f32[256]{0:T(256)}, u32[]{:S(2)}) copy-start(f32[256]{0:T(256)} %param.17) | copy-start | bytes 3076
  3.6 2.6 %copy-start.2 = (bf16[256,256]{1,0:T(8,128)(2,1)S(1)}, bf16[256,256]{1,0:T(8,128)(2,1)}, u32[]{:S(2)}) copy-start(bf16[256,256]{1,0:T(8,128)(2,1)} %param.18) | copy-start | bytes 393220
  3.6 3.4 %copy-start.3 = (bf16[256,256]{1,0:T(8,128)(2,1)S(1)}, bf16[256,256]{1,0:T(8,128)(2,1)}, u32[]{:S(2)}) copy-start(bf16[256,256]{1,0:T(8,128)(2,1)} %param.19) | copy-start | bytes 393220

commit v2 on v1

--- a/solution.py
+++ b/solution.py
@@ -11,6 +11,7 @@
 UNROTATED_WIDTH = 64
 ROPE = 32
 LANES = 128
+CHUNKS = 4
 
 rope_base = 10000.0
 epsilon = 1e-06
@@ -63,49 +64,66 @@
 
 
 def attention_kernel(
-    n, heads, scale, q_ref, x_ref, wk_ref, wv_ref, wo_ref, wu_ref,
+    n, n_tp, heads, scale, q_ref, x_ref, wk_ref, wv_ref, wo_ref, wu_ref,
     part_ref, full_ref,
-    xs, peak, acc, xsend, xrecv, wsend, wrecv, own_sem,
+    xs, peak, acc, xsend, xrecv, ssend, srecv, wsend, wrecv, own_sem,
 ):
     at = ring_ids(n)
     tp = lax.axis_index("tp")
     me = lax.axis_index("sp")
     to = ((at(1), tp), (at(-1), tp))
+    peers = [(tp + k) % n_tp for k in range(1, n_tp)]
+    onward = (at(1 - 2 * (tp % 2)), tp)
     barrier = pltpu.get_barrier_semaphore()
-    for target in to:
+    for target in list(to) + [(me, p) for p in peers]:
         pl.semaphore_signal(barrier, inc=1, device_id=target, device_id_type=MESH)
-    pl.semaphore_wait(barrier, 2)
+    pl.semaphore_wait(barrier, 2 + n_tp - 1)
 
     latent = wk_ref.shape[1]
     value_width = wv_ref.shape[0] // heads
 
-    def x_copy(step, half, src):
-        return pltpu.make_async_remote_copy(
-            src_ref=src, dst_ref=xs.at[step + 1, half],
-            send_sem=xsend.at[step, half], recv_sem=xrecv.at[step, half],
+    def x_copy(step, src):
+        return pltpu.make_async_remote_copy(
+            src_ref=src, dst_ref=xs.at[step + 1, tp],
+            send_sem=xsend.at[step], recv_sem=xrecv.at[step],
+            device_id=onward, device_id_type=MESH,
+        )
+
+    def share(step, k):
+        return pltpu.make_async_remote_copy(
+            src_ref=xs.at[step, tp], dst_ref=xs.at[step, tp],
+            send_sem=ssend.at[step, k], recv_sem=srecv.at[step, k],
+            device_id=(me, peers[k]), device_id_type=MESH,
+        )
+
+    def share_wait(step):
+        for k in range(n_tp - 1):
+            pltpu.make_async_remote_copy(
+                src_ref=xs.at[step, tp], dst_ref=xs.at[step, (tp + n_tp - 1 - k) % n_tp],
+                send_sem=ssend.at[step, k], recv_sem=srecv.at[step, k],
+                device_id=(me, peers[k]), device_id_type=MESH,
+            ).wait_recv()
+
+    def w_copy(step, half, c, first):
+        owner = at(-step) if half == 0 else at(step)
+        return pltpu.make_async_remote_copy(
+            src_ref=wu_ref.at[half, c] if first else full_ref.at[owner, half, c],
+            dst_ref=full_ref.at[owner, half, c],
+            send_sem=wsend.at[step, half, c], recv_sem=wrecv.at[step, half, c],
             device_id=to[half], device_id_type=MESH,
         )
 
-    def w_copy(step, half, src):
-        owner = at(-step) if half == 0 else at(step)
-        return pltpu.make_async_remote_copy(
-            src_ref=full_ref.at[owner, half] if src is None else src,
-            dst_ref=full_ref.at[owner, half],
-            send_sem=wsend.at[step, half], recv_sem=wrecv.at[step, half],
-            device_id=to[half], device_id_type=MESH,
-        )
-
-    for half in range(2):
-        x_copy(0, half, x_ref.at[half]).start()
-    for half in range(2):
-        w_copy(0, half, wu_ref.at[half]).start()
+    x_copy(0, x_ref.at[tp]).start()
+    for c in range(CHUNKS):
+        for half in range(2):
+            w_copy(0, half, c, True).start()
     own = pltpu.make_async_copy(wu_ref, full_ref.at[me], own_sem)
     own.start()
     peak[...] = jnp.full(peak.shape, -1e30, F32)
     acc[...] = jnp.zeros(acc.shape, F32)
 
-    def attend(block_a, block_b):
-        block = jnp.concatenate([block_a, block_b], axis=1)
+    def attend(blocks):
+        block = jnp.concatenate(blocks, axis=1)
         lat = block[:latent]
         rot = block[latent:]
         keys = block.shape[1]
@@ -127,27 +145,34 @@
                 p, v_h, NT, preferred_element_type=F32)
             peak[h] = new
 
-    attend(x_ref[0], x_ref[1])
-
     def turn(i, carry):
-        for half in range(2):
-            x_copy(i - 1, half, x_ref.at[half]).wait_recv()
-
-            @pl.when(i < n - 1)
-            def _():
-                x_copy(i, half, xs.at[i, half]).start()
-
-        for half in range(2):
-            w_copy(i - 1, half, wu_ref.at[half]).wait_recv()
-
-            @pl.when(i < n - 1)
-            def _():
-                w_copy(i, half, None).start()
-
-        attend(xs[i, 0], xs[i, 1])
+        x_copy(i - 1, x_ref.at[tp]).wait_recv()
+
+        @pl.when(i < n - 1)
+        def _():
+            x_copy(i, xs.at[i, tp]).start()
+
+        for k in range(n_tp - 1):
+            share(i, k).start()
+        for c in range(CHUNKS):
+            for half in range(2):
+                w_copy(i - 1, half, c, True).wait_recv()
+
+                @pl.when(i < n - 1)
+                def _():
+                    w_copy(i, half, c, False).start()
+
+        @pl.when(i > 1)
+        def _():
+            share_wait(i - 1)
+            attend([xs[i - 1, t] for t in range(n_tp)])
+
         return carry
 
+    attend([x_ref[t] for t in range(n_tp)])
     lax.fori_loop(1, n, turn, 0)
+    share_wait(n - 1)
+    attend([xs[n - 1, t] for t in range(n_tp)])
 
     width = part_ref.shape[2]
     group = []
@@ -163,18 +188,21 @@
     own.wait()
 
     def drain(i, carry):
-        for half in range(2):
-            x_copy(i, half, x_ref.at[half]).wait_send()
-            w_copy(i, half, wu_ref.at[half]).wait_send()
+        x_copy(i, x_ref.at[tp]).wait_send()
+        for k in range(n_tp - 1):
+            share(i + 1, k).wait_send()
+        for c in range(CHUNKS):
+            for half in range(2):
+                w_copy(i, half, c, True).wait_send()
         return carry
 
     lax.fori_loop(0, n - 1, drain, 0)
 
 
 def feed_kernel(
-    n, n_tp, narrow, part_ref, res_ref, gain_ref, up_hbm, wd_ref,
+    n, n_tp, narrow, part_ref, res_hbm, gain_ref, up_hbm, wd_hbm,
     out_ref,
-    up, down, parts, ys, sq, own_stream, hidden, pieces, fin,
+    res_ref, up, down, parts, ys, sq, own_stream, hidden, pieces, fin,
     dsend, drecv, psend, precv, ysend, yrecv, qsend, qrecv, fsend, frecv, local,
 ):
     at = ring_ids(n)
@@ -190,11 +218,24 @@
     rows, width = res_ref.shape
     per = n // n_tp
 
-    def d_copy(step, half, src):
-        return pltpu.make_async_remote_copy(
-            src_ref=down.at[step, half] if src is None else src,
-            dst_ref=down.at[step + 1, half],
-            send_sem=dsend.at[step, half], recv_sem=drecv.at[step, half],
+    lines = down.shape[2] // CHUNKS
+
+    def own_half(half):
+        if narrow:
+            return wd_hbm.at[half]
+        return wd_hbm.at[:, half * down.shape[3]:(half + 1) * down.shape[3]]
+
+    def d_copy(step, half, c, first):
+        span = pl.ds(c * lines, lines)
+        if not first:
+            src = down.at[step, half, span]
+        elif narrow:
+            src = wd_hbm.at[half, span]
+        else:
+            src = wd_hbm.at[span, half * down.shape[3]:(half + 1) * down.shape[3]]
+        return pltpu.make_async_remote_copy(
+            src_ref=src, dst_ref=down.at[step + 1, half, span],
+            send_sem=dsend.at[step, half, c], recv_sem=drecv.at[step, half, c],
             device_id=to[half], device_id_type=MESH,
         )
 
@@ -220,39 +261,51 @@
             device_id=(sp, peers[k]), device_id_type=MESH,
         )
 
-    def event(step):
+    def landed(step, c):
         for half in range(2):
-            d_copy(step - 1, half, wd_ref.at[half]).wait_recv()
-            d_copy(step, half, None).start()
-
-    for half in range(2):
-        d_copy(0, half, wd_ref.at[half]).start()
+            d_copy(step, half, c, True).wait_recv()
+
+    def event(step, c):
+        landed(step - 1, c)
+        for half in range(2):
+            d_copy(step, half, c, False).start()
+
+    def events(first, last):
+        for tick in range(first, last):
+            event(1 + tick // CHUNKS, tick % CHUNKS)
+
+    for c in range(CHUNKS):
+        for half in range(2):
+            d_copy(0, half, c, True).start()
     for k in range(n_tp - 1):
         p_copy(k).start()
-    load = pltpu.make_async_copy(up_hbm, up, local.at[0])
-    load.start()
-    early = min(n - 2, 5)
-
-    def maybe(step):
-        if step <= early:
-            event(step)
-
-    maybe(1)
+    loads = [
+        pltpu.make_async_copy(
+            res_hbm.at[:, pl.ds(pl.multiple_of(tp * width, LANES), width)], res_ref, local.at[0]),
+        pltpu.make_async_copy(up_hbm, up, local.at[1]),
+        pltpu.make_async_copy(own_half(0), down.at[0, 0], local.at[2]),
+        pltpu.make_async_copy(own_half(1), down.at[0, 1], local.at[3]),
+    ]
+    for load in loads:
+        load.start()
+
+    early = 4
+    events(0, 6)
     for k in range(n_tp - 1):
         p_copy(k).wait_recv()
-    maybe(2)
+    loads[0].wait()
     stream = part_ref[tp].astype(F32)
     for k in range(n_tp - 1):
         stream = stream + parts[k].astype(F32)
     stream = stream + res_ref[...].astype(F32)
     own_stream[...] = stream
-    ys[tp] = (stream * gain_ref[...]).astype(BF16)
+    ys[tp] = (stream * gain_ref[tp]).astype(BF16)
     total = jnp.sum(stream * stream, axis=1, keepdims=True)
     sq[0] = jnp.transpose(jnp.broadcast_to(total, (rows, LANES)))[:8]
     for k in range(n_tp - 1):
         q_copy(k).start()
         y_copy(k).start()
-    maybe(3)
+    events(6, 12)
     for k in range(n_tp - 1):
         q_copy(k).wait_recv()
     for k in range(n_tp - 1):
@@ -261,13 +314,12 @@
             send_sem=ysend.at[k], recv_sem=yrecv.at[k],
             device_id=(sp, peers[k]), device_id_type=MESH,
         ).wait_recv()
-    maybe(4)
     squares = sq[0]
     for k in range(1, n_tp):
         squares = squares + sq[k]
     squares = jnp.concatenate([squares] * (LANES // 8), axis=0)
     factor = lax.rsqrt(jnp.transpose(squares)[:, :1] / (width * n_tp) + epsilon)
-    load.wait()
+    loads[1].wait()
     units = hidden.shape[1]
     tile = math.gcd(units, 512)
 
@@ -279,10 +331,14 @@
                 ys[t], up[t * width:(t + 1) * width, columns], preferred_element_type=F32)
         total = jnp.maximum(total, 0.0) * factor
         hidden[:, columns] = (total * total).astype(BF16)
+
+        @pl.when(c < CHUNKS)
+        def _():
+            event(early, c)
+
         return carry
 
     lax.fori_loop(0, units // tile, up_step, 0)
-    maybe(5)
 
     def owners(i):
         return at(-i), at(i)
@@ -317,18 +373,24 @@
             def _():
                 fin[tp, owner % per, half] = pieces[i, half]
 
-    down_block(0, wd_ref[0], wd_ref[1])
+    for load in loads[2:]:
+        load.wait()
+    down_block(0, down[0, 0], down[0, 1])
 
     def down_step(i, carry):
-        @pl.when(i > early)
+        @pl.when(i <= CHUNKS)
         def _():
-            for half in range(2):
-                d_copy(i - 1, half, wd_ref.at[half]).wait_recv()
-
-        @pl.when(jnp.logical_and(i > early, i < n - 1))
+            event(early + 1, i - 1)
+
+        @pl.when(i > early + 1)
         def _():
-            for half in range(2):
-                d_copy(i, half, None).start()
+            for c in range(CHUNKS):
+                landed(i - 1, c)
+
+                @pl.when(i < n - 1)
+                def _():
+                    for half in range(2):
+                        d_copy(i, half, c, False).start()
 
         down_block(i, down[i, 0], down[i, 1])
         return carry
@@ -355,8 +417,9 @@
             out_ref[:, start:start + piece] = (total + mixed).astype(BF16)
 
     def drain(i, carry):
-        for half in range(2):
-            d_copy(i, half, wd_ref.at[half]).wait_send()
+        for c in range(CHUNKS):
+            for half in range(2):
+                d_copy(i, half, c, True).wait_send()
         return carry
 
     lax.fori_loop(0, n - 1, drain, 0)
@@ -421,51 +484,55 @@
     key_rot = rotate(rope_keys.astype(F32), phases).astype(BF16)
     x = jnp.concatenate([lat_norm, key_rot], axis=1)
     wide = x.shape[1]
-    x = jnp.transpose(x.reshape(2, rows // 2, wide), (0, 2, 1))
+    x = jnp.transpose(x.reshape(n_tp, rows // n_tp, wide), (0, 2, 1))
 
     width = model // n_tp
     depth, units = w_up.shape
     dma = pltpu.SemaphoreType.DMA
     part, full = pl.pallas_call(
         functools.partial(
-            attention_kernel, n, heads,
+            attention_kernel, n, n_tp, heads,
             math.log2(math.e) / math.sqrt(UNROTATED_WIDTH + ROPE)),
         out_shape=(
             jax.ShapeDtypeStruct((n_tp, rows, width), BF16),
-            jax.ShapeDtypeStruct((n, 2, depth // 2, units), BF16),
+            jax.ShapeDtypeStruct((n, 2, CHUNKS, depth // 2 // CHUNKS, units), BF16),
         ),
         in_specs=[vmem()] * 5 + [hbm()],
         out_specs=(vmem(), hbm()),
         scratch_shapes=[
-            pltpu.VMEM((n, 2, wide, rows // 2), BF16),
+            pltpu.VMEM((n, n_tp, wide, rows // n_tp), BF16),
             pltpu.VMEM((heads, rows, 1), F32),
             pltpu.VMEM((heads, rows, LANES), F32),
-            dma((n - 1, 2)), dma((n - 1, 2)), dma((n - 1, 2)), dma((n - 1, 2)), dma,
+            dma((n - 1,)), dma((n - 1,)),
+            dma((n, n_tp - 1)), dma((n, n_tp - 1)),
+            dma((n - 1, 2, CHUNKS)), dma((n - 1, 2, CHUNKS)), dma,
         ],
         compiler_params=pltpu.CompilerParams(
             collective_id=0, has_side_effects=True, vmem_limit_bytes=56 * 2**20),
         name="attend",
     )(
         queries, x, jnp.transpose(key_up_weight), jnp.transpose(value_up_weight),
-        w_out, w_up.reshape(2, depth // 2, units),
+        w_out, w_up.reshape(2, CHUNKS, depth // 2 // CHUNKS, units),
     )
 
     hidden_units, share = w_down.shape
     narrow = (share // 2) % LANES != 0
-    halves = jnp.transpose(
-        w_down.reshape(hidden_units, 2, share // 2), (1, 2, 0) if narrow else (1, 0, 2))
-    t = lax.axis_index("tp")
-    own_residual = lax.dynamic_slice_in_dim(residual_in, t * width, width, 1)
-    own_gain = lax.dynamic_slice_in_dim(norm_gain, t * width, width, 0)[None, :]
+    if narrow:
+        down_in = jnp.transpose(w_down.reshape(hidden_units, 2, share // 2), (1, 2, 0))
+        half_shape = (share // 2, hidden_units)
+    else:
+        down_in = w_down
+        half_shape = (hidden_units, share // 2)
     per = n // n_tp
     return pl.pallas_call(
         functools.partial(feed_kernel, n, n_tp, narrow),
         out_shape=jax.ShapeDtypeStruct((rows, width), BF16),
-        in_specs=[vmem()] * 3 + [hbm(), vmem()],
+        in_specs=[vmem(), hbm(), vmem(), hbm(), hbm()],
         out_specs=vmem(),
         scratch_shapes=[
+            pltpu.VMEM((rows, width), BF16),
             pltpu.VMEM((model, units), BF16),
-            pltpu.VMEM((n,) + halves.shape, BF16),
+            pltpu.VMEM((n, 2) + half_shape, BF16),
             pltpu.VMEM((n_tp - 1, rows, width), BF16),
             pltpu.VMEM((n_tp, rows, width), BF16),
             pltpu.VMEM((n_tp, 8, rows), F32),
@@ -473,17 +540,17 @@
             pltpu.VMEM((rows, units), BF16),
             pltpu.VMEM((n, 2, rows, share // 2), BF16),
             pltpu.VMEM((n_tp, per, 2, rows, share // 2), BF16),
-            dma((n - 1, 2)), dma((n - 1, 2)),
+            dma((n - 1, 2, CHUNKS)), dma((n - 1, 2, CHUNKS)),
             dma((n_tp - 1,)), dma((n_tp - 1,)),
             dma((n_tp - 1,)), dma((n_tp - 1,)),
             dma((n_tp - 1,)), dma((n_tp - 1,)),
             dma((n, 2)), dma((n_tp, per, 2)),
-            dma((1,)),
+            dma((4,)),
         ],
         compiler_params=pltpu.CompilerParams(
             collective_id=1, has_side_effects=True, vmem_limit_bytes=60 * 2**20),
         name="feed",
-    )(part, own_residual, own_gain, full.reshape(model, units), halves)
+    )(part, residual_in, norm_gain.reshape(n_tp, 1, width), full.reshape(model, units), down_in)
 
 
 def solution(mesh):

time: 230 us -> 205 us (0.89)
  Pallas kernels: 215 us -> 195 us
  local copies, waits for them, and re-layouts: 12.7 us -> 7.69 us
    pallas_call x1, Pallas kernels: 114 us -> 102 us  [on_device(): pl.pallas_call(functools.partial(attention_kernel, n, n_tp, heads, math.l...]
    pallas_call x1, Pallas kernels: 102 us -> 92.2 us  [on_device(): pl.pallas_call(functools.partial(feed_kernel, n, n_tp, narrow), out_shape...]
    unnamed x16 -> x13, local copies, waits for them, and re-layouts: 7 us -> 5.46 us
where the time goes in v2:
time: 205 us
  Pallas kernels  195 us (95%)
  local copies, waits for them, and re-layouts  7.69 us (4%)
  other arithmetic  2.57 us (1%)
    pallas_call x1, Pallas kernels, on_device(): pl.pallas_call(functools.partial(attention_kernel, n, n_tp, heads, math.l...  102 us
    pallas_call x1, Pallas kernels, on_device(): pl.pallas_call(functools.partial(feed_kernel, n, n_tp, narrow), out_shape...  92.2 us
    unnamed x13, local copies, waits for them, and re-layouts  5.46 us

profile of v2, /device:TPU:0, one launch (start us, length us, event | category | flops | bytes accessed | tf_op | source)
XLA Modules:
  0.0 205.0 jit_solution(13552784738457386569)
XLA Ops:
  0.0 0.0 copy-start
  0.0 0.0 copy-start.2
  0.0 0.0 copy-start.3
  0.0 0.1 pad.6.clone
  0.1 1.1 fusion
  1.3 0.8 convert_element_type.22
  2.0 0.0 copy-start.1
  2.0 0.2 subtract_convert_fusion.1
  2.2 0.1 copy.22
  2.4 0.1 copy.23
  2.5 1.0 copy.20
  3.6 1.7 copy.26
  5.3 0.0 copy-done.2
  5.3 0.8 copy.27
  6.0 0.0 copy-done
  6.0 0.0 copy-done.3
  6.0 0.1 fusion.2
  6.2 0.1 pad_maximum_fusion
  6.3 0.9 copy.25
  7.2 0.0 copy-done.1
  7.2 0.1 copy.19
  7.3 0.1 maximum_maximum_fusion
  7.5 1.0 copy.28.q_ref
  8.5 102.4 %attend.1 = (bf16[4,512,512]{2,1,0:T(8,128)(2,1)}, bf16[8,2,4,32,2048]{4,3,2,1,0:T(8,128)(2,1)}) custom-call(bf16[512,512]{1,0:T(8,128)(2,1)} %copy.28.q_ref, bf16[4,288,128]{2,1,0:T(8,128)(2,1)} %bitcast.14, bf16[256,256]{1,0:T(8,128)(2,1)} %bitcast.17, bf16[256,256]{1,0:T(8,128)(2,1)} %bitcast.18, bf16[256,2048]{1,0:T(8,128)(2,1)} %wo_ref.1, ...), custom_call_target="tpu_custom_call" | custom-call | tf_op jit(solution)/shard_map/attend/pallas_call | solution.py:492
  110.9 92.2 %feed.1 = bf16[512,512]{1,0:T(8,128)(2,1)} custom-call(bf16[4,512,512]{2,1,0:T(8,128)(2,1)} %get-tuple-element.7.part_ref, bf16[512,2048]{1,0:T(8,128)(2,1)} %res_hbm.1, f32[4,1,512]{2,1,0:T(1,128)} %bitcast.20, bf16[2048,2048]{1,0:T(8,128)(2,1)} %bitcast.11, bf16[2048,256]{1,0:T(8,128)(2,1)} %wd_hbm.1), custom_call_target="tpu_custom_call" | custom-call | tf_op jit(solution)/shard_map/feed/pallas_call | solution.py:527
  203.1 1.9 copy.32
  (6 shorter events, 0.1 us)
Async XLA Ops:
  0.0 6.0 %copy-start = (bf16[512,256]{1,0:T(8,128)(2,1)S(1)}, bf16[512,256]{1,0:T(8,128)(2,1)}, u32[]{:S(2)}) copy-start(bf16[512,256]{1,0:T(8,128)(2,1)} %param.15) | copy-start | bytes 786436
  0.0 5.3 %copy-start.2 = (bf16[256,256]{1,0:T(8,128)(2,1)S(1)}, bf16[256,256]{1,0:T(8,128)(2,1)}, u32[]{:S(2)}) copy-start(bf16[256,256]{1,0:T(8,128)(2,1)} %param.19) | copy-start | bytes 393220
  0.0 6.0 %copy-start.3 = (f32[256]{0:T(256)S(1)}, f32[256]{0:T(256)}, u32[]{:S(2)}) copy-start(f32[256]{0:T(256)} %param.17) | copy-start | bytes 3076
  2.0 5.2 %copy-start.1 = (bf16[512,256]{1,0:T(8,128)(2,1)S(1)}, bf16[512,256]{1,0:T(8,128)(2,1)}, u32[]{:S(2)}) copy-start(bf16[512,256]{1,0:T(8,128)(2,1)} %param.13) | copy-start | bytes 786436

commit v3 on v2

--- a/solution.py
+++ b/solution.py
@@ -64,9 +64,9 @@
 
 
 def attention_kernel(
-    n, n_tp, heads, scale, q_ref, x_ref, wk_ref, wv_ref, wo_ref, wu_ref,
+    n, n_tp, heads, scale, q_ref, x_ref, wk_in, wv_in, wo_ref, wu_ref,
     part_ref, full_ref,
-    xs, peak, acc, xsend, xrecv, ssend, srecv, wsend, wrecv, own_sem,
+    wk_ref, wv_ref, xs, peak, acc, xsend, xrecv, ssend, srecv, wsend, wrecv, own_sem,
 ):
     at = ring_ids(n)
     tp = lax.axis_index("tp")
@@ -119,6 +119,8 @@
             w_copy(0, half, c, True).start()
     own = pltpu.make_async_copy(wu_ref, full_ref.at[me], own_sem)
     own.start()
+    wk_ref[...] = jnp.transpose(wk_in[...].astype(F32)).astype(BF16)
+    wv_ref[...] = jnp.transpose(wv_in[...].astype(F32)).astype(BF16)
     peak[...] = jnp.full(peak.shape, -1e30, F32)
     acc[...] = jnp.zeros(acc.shape, F32)
 
@@ -147,20 +149,13 @@
 
     def turn(i, carry):
         x_copy(i - 1, x_ref.at[tp]).wait_recv()
-
-        @pl.when(i < n - 1)
-        def _():
-            x_copy(i, xs.at[i, tp]).start()
-
+        x_copy(i, xs.at[i, tp]).start()
         for k in range(n_tp - 1):
             share(i, k).start()
         for c in range(CHUNKS):
             for half in range(2):
                 w_copy(i - 1, half, c, True).wait_recv()
-
-                @pl.when(i < n - 1)
-                def _():
-                    w_copy(i, half, c, False).start()
+                w_copy(i, half, c, False).start()
 
         @pl.when(i > 1)
         def _():
@@ -170,9 +165,17 @@
         return carry
 
     attend([x_ref[t] for t in range(n_tp)])
-    lax.fori_loop(1, n, turn, 0)
-    share_wait(n - 1)
-    attend([xs[n - 1, t] for t in range(n_tp)])
+    lax.fori_loop(1, n - 1, turn, 0)
+    x_copy(n - 2, x_ref.at[tp]).wait_recv()
+    for k in range(n_tp - 1):
+        share(n - 1, k).start()
+
+    def last(i, carry):
+        share_wait(i)
+        attend([xs[i, t] for t in range(n_tp)])
+        return carry
+
+    lax.fori_loop(n - 2, n, last, 0)
 
     width = part_ref.shape[2]
     group = []
@@ -186,6 +189,9 @@
         ).astype(BF16)
 
     own.wait()
+    for c in range(CHUNKS):
+        for half in range(2):
+            w_copy(n - 2, half, c, True).wait_recv()
 
     def drain(i, carry):
         x_copy(i, x_ref.at[tp]).wait_send()
@@ -500,6 +506,8 @@
         in_specs=[vmem()] * 5 + [hbm()],
         out_specs=(vmem(), hbm()),
         scratch_shapes=[
+            pltpu.VMEM(key_up_weight.shape[::-1], BF16),
+            pltpu.VMEM(value_up_weight.shape[::-1], BF16),
             pltpu.VMEM((n, n_tp, wide, rows // n_tp), BF16),
             pltpu.VMEM((heads, rows, 1), F32),
             pltpu.VMEM((heads, rows, LANES), F32),
@@ -511,7 +519,7 @@
             collective_id=0, has_side_effects=True, vmem_limit_bytes=56 * 2**20),
         name="attend",
     )(
-        queries, x, jnp.transpose(key_up_weight), jnp.transpose(value_up_weight),
+        queries, x, key_up_weight, value_up_weight,
         w_out, w_up.reshape(2, CHUNKS, depth // 2 // CHUNKS, units),
     )
 

time: 205 us -> 201 us (0.980)
  Pallas kernels: 195 us -> 192 us
  local copies, waits for them, and re-layouts: 7.69 us -> 5.28 us
    pallas_call x1, Pallas kernels: 102 us -> 99.5 us  [on_device(): pl.pallas_call(functools.partial(attention_kernel, n, n_tp, heads, math.l...]
    unnamed x13 -> x7, local copies, waits for them, and re-layouts: 5.46 us -> 3.03 us
where the time goes in v3:
time: 201 us
  Pallas kernels  192 us (96%)
  local copies, waits for them, and re-layouts  5.28 us (3%)
  other arithmetic  3.27 us (2%)
    pallas_call x1, Pallas kernels, on_device(): pl.pallas_call(functools.partial(attention_kernel, n, n_tp, heads, math.l...  99.5 us
    pallas_call x1, Pallas kernels, on_device(): pl.pallas_call(functools.partial(feed_kernel, n, n_tp, narrow), out_shape...  92.6 us

profile of v3, /device:TPU:0, one launch (start us, length us, event | category | flops | bytes accessed | tf_op | source)
XLA Modules:
  0.0 200.8 jit_solution(16645802762042753335)
XLA Ops:
  0.0 0.0 copy-start
  0.0 0.0 copy-start.1
  0.0 0.1 pad.6.clone
  0.1 1.1 fusion
  1.3 0.8 convert_element_type.22
  2.0 0.2 subtract_convert_fusion.1
  2.2 0.1 copy.20
  2.4 0.1 copy.21
  2.5 1.0 copy.18
  3.6 0.0 copy-done
  3.6 0.8 fusion.2
  4.4 0.1 pad_maximum_fusion
  4.5 0.9 copy.23
  5.5 0.0 copy-done.1
  5.5 0.1 copy.17
  5.6 0.1 maximum_maximum_fusion
  5.8 1.0 copy.24.q_ref
  6.8 99.5 %attend.1 = (bf16[4,512,512]{2,1,0:T(8,128)(2,1)}, bf16[8,2,4,32,2048]{4,3,2,1,0:T(8,128)(2,1)}) custom-call(bf16[512,512]{1,0:T(8,128)(2,1)} %copy.24.q_ref, bf16[4,288,128]{2,1,0:T(8,128)(2,1)} %bitcast.12, bf16[256,256]{1,0:T(8,128)(2,1)} %wk_in.1, bf16[256,256]{1,0:T(8,128)(2,1)} %wv_in.1, bf16[256,2048]{1,0:T(8,128)(2,1)} %wo_ref.1, ...), custom_call_target="tpu_custom_call" | custom-call | tf_op jit(solution)/shard_map/attend/pallas_call | solution.py:498
  106.3 92.6 %feed.1 = bf16[512,512]{1,0:T(8,128)(2,1)} custom-call(bf16[4,512,512]{2,1,0:T(8,128)(2,1)} %get-tuple-element.7.part_ref, bf16[512,2048]{1,0:T(8,128)(2,1)} %res_hbm.1, f32[4,1,512]{2,1,0:T(1,128)} %bitcast.16, bf16[2048,2048]{1,0:T(8,128)(2,1)} %bitcast.9, bf16[2048,256]{1,0:T(8,128)(2,1)} %wd_hbm.1), custom_call_target="tpu_custom_call" | custom-call | tf_op jit(solution)/shard_map/feed/pallas_call | solution.py:535
  198.9 1.9 copy.28
  (6 shorter events, 0.1 us)
Async XLA Ops:
  0.0 3.6 %copy-start = (bf16[512,256]{1,0:T(8,128)(2,1)S(1)}, bf16[512,256]{1,0:T(8,128)(2,1)}, u32[]{:S(2)}) copy-start(bf16[512,256]{1,0:T(8,128)(2,1)} %param.15) | copy-start | bytes 786436
  0.0 5.5 %copy-start.1 = (bf16[512,256]{1,0:T(8,128)(2,1)S(1)}, bf16[512,256]{1,0:T(8,128)(2,1)}, u32[]{:S(2)}) copy-start(bf16[512,256]{1,0:T(8,128)(2,1)} %param.13) | copy-start | bytes 786436
